TPU v7x, 128 devices: a whole 4x4x4 slice. The times are simulated.
128 devices in a mesh: fs: 16 (over z, y), tp: 8 (over x, core).
Axes of the slice: x: 4, y: 4, z: 4, core: 2. Of those that a mesh axis runs over, the one named last changes fastest.
Arguments:
- tokens: bfloat16 [16384, 2048], P('fs', 'tp'), may hold values from -6 to 6
- norm_gain: float32 [2048], P('fs'), may hold values from 0.1 to 1.9
- up_master: float32 [2048, 8192], P('fs', 'tp'), may hold values from -0.125 to 0.125
- down_master: float32 [2048, 8192], P('fs', 'tp'), may hold values from -0.0625 to 0.0625
Outputs:
- up_weights: bfloat16 [2048, 8192], P(None, 'tp')
- down_weights: bfloat16 [8192, 2048], P('tp')
- mlp_out: bfloat16 [16384, 2048], P('fs', 'tp')
All inputs are finite; a program needn't handle non-finite values.
Results may differ from a plain program's by a relative error of at most 0.014.
Values may be sent and summed in bfloat16 or wider, within the bound.
A program may use at most 128 MiB of HBM per device.

v0:
```python
import jax
import jax.numpy as jnp
from jax import lax
from jax.sharding import PartitionSpec as P

norm_floor = 1e-06


def side_by_side(arrays, axis, dim, along):
    ends, at = ([], 0)
    for a in arrays[:-1]:
        at += a.shape[along]
        ends.append(at)
    both = jnp.concatenate(arrays, axis=along)
    return tuple(jnp.split(lax.all_gather(both, axis, axis=dim, tiled=True), ends, axis=along))


def on_device(tokens, norm_gain, up_master, down_master):
    up_local = (norm_gain[:, None] * up_master).astype(jnp.bfloat16)
    down_local = down_master.astype(jnp.bfloat16)
    gathered = lax.all_gather(tokens, "tp", axis=1, tiled=True)
    widened = gathered.astype(jnp.float32)
    normed = (
        widened * lax.rsqrt(jnp.mean(widened * widened, axis=-1, keepdims=True) + norm_floor)
    ).astype(jnp.bfloat16)
    up_whole, down_whole = side_by_side((up_local, down_local), "fs", 0, 1)
    preact = jnp.dot(normed, up_whole, preferred_element_type=jnp.float32)
    hidden = jnp.square(jax.nn.relu(preact)).astype(jnp.bfloat16)
    partial_value = jnp.einsum("tf,df->td", hidden, down_whole, preferred_element_type=jnp.float32)
    summed = lax.psum_scatter(
        partial_value.astype(jnp.bfloat16), "tp", scatter_dimension=1, tiled=True
    )
    return (up_whole, jnp.transpose(down_whole), summed)


def solution(mesh):
    in_specs = (P("fs", "tp"), P("fs"), P("fs", "tp"), P("fs", "tp"))
    out_specs = (P(None, "tp"), P("tp", None), P("fs", "tp"))
    return jax.shard_map(
        on_device, mesh=mesh, in_specs=in_specs, out_specs=out_specs, check_vma=False
    )
```

profile of v0, /device:TPU:0, one launch (start us, length us, event | category | flops | bytes accessed | tf_op | source)
XLA Modules:
  0.0 186.4 jit_solution(12943971067631530127)
XLA Ops:
  7.2 0.0 all-gather.5.cloned.1.call-start
  7.2 0.7 all-gather.5.cloned.1.call-update
  7.9 0.0 all-gather.3.cloned.1.call-start
  7.9 1.2 copy.7
  9.2 1.2 copy.8
  10.4 0.7 multiply_convert_fusion.2
  11.1 0.8 pad_maximum_fusion
  11.9 0.0 all-gather.3.cloned.1.call-update
  12.0 0.0 reduce-scatter.2.cloned.1.call-start
  12.0 35.6 %all-gather.5.cloned.1.call-done = bf16[1024,2048]{1,0:T(8,128)(2,1)} async-done(((bf16[1024,256]{1,0:T(8,128)(2,1)}), bf16[1024,2048]{1,0:T(8,128)(2,1)}) %all-gather.5.cloned.1.call-update) | async-done | bytes 4194320 | tf_op jit(solution)/shard_map/all_gather | solution.py:21
  47.7 3.1 %fusion = f32[1024]{0:T(1024)S(1)} fusion(bf16[1024,2048]{1,0:T(8,128)(2,1)} %all-gather.5.cloned.1.call-done), kind=kLoop, calls=%fused_computation.2 | loop fusion | flops 6290432 | bytes 4198400 | tf_op jit(solution)/shard_map/reduce_sum | solution.py:24
  50.7 78.0 %all-gather.3.cloned.1.call-done = bf16[2048,2048]{0,1:T(8,128)(2,1)} async-done(((bf16[128,2048]{0,1:T(8,128)(2,1)}), bf16[2048,2048]{0,1:T(8,128)(2,1)}) %all-gather.3.cloned.1.call-update) | async-done | bytes 8388624 | tf_op jit(solution)/shard_map/all_gather | solution.py:15
  128.7 0.0 copy-start
  128.7 7.7 %fusion.2 = f32[1024,1024]{1,0:T(8,128)S(1)} fusion(bf16[1024,2048]{1,0:T(8,128)(2,1)} %all-gather.5.cloned.1.call-done, f32[1024]{0:T(1024)S(1)} %add_rsqrt_fusion, bf16[2048,2048]{0,1:T(8,128)(2,1)} %all-gather.3.cloned.1.call-done), kind=kOutput, calls=%fused_computation.4 | convolution fusion | flops 4301258752 | bytes 12587008 | tf_op jit(solution)/shard_map/dot_general | solution.py:27
  136.5 0.0 copy-done
  136.5 6.1 %convolution_convert_fusion = bf16[1024,2048]{1,0:T(8,128)(2,1)} fusion(bf16[2048,2048]{0,1:T(8,128)(2,1)S(1)} %copy-done, f32[1024,1024]{1,0:T(8,128)S(1)} %fusion.2), kind=kOutput, calls=%fused_computation.7 | convolution fusion | flops 4300210176 | bytes 12582912 | tf_op jit(solution)/shard_map/tf,df->td/dot_general | solution.py:29
  142.6 0.0 reduce-scatter.2.cloned.1.call-update
  142.6 6.2 %slice_bitcast_fusion = (bf16[1024,2048]{1,0:T(8,128)(2,1)}, bf16[2048,1024]{0,1:T(8,128)(2,1)}) fusion(bf16[2048,2048]{0,1:T(8,128)(2,1)} %all-gather.3.cloned.1.call-done), kind=kLoop, calls=%fused_computation.9 | loop fusion | bytes 16777216 | tf_op jit(solution)/shard_map/transpose | solution.py:33
  148.7 6.4 %copy.9 = bf16[2048,1024]{1,0:T(8,128)(2,1)} copy(bf16[2048,1024]{0,1:T(8,128)(2,1)} %get-tuple-element.7) | data formatting | bytes 8388608
  155.2 24.7 %reduce-scatter.2.cloned.1.call-done = bf16[1024,256]{1,0:T(8,128)(2,1)} async-done(((bf16[1024,2048]{1,0:T(8,128)(2,1)}), bf16[1024,256]{1,0:T(8,128)(2,1)}) %reduce-scatter.2.cloned.1.call-update) | async-done | bytes 524304 | tf_op jit(solution)/shard_map/reduce_scatter | solution.py:30
  (1 shorter events, 0.0 us)
Async XLA Ops:
  7.2 40.5 %all-gather.5.cloned.1.call-start = ((), (), s32[]{:S(2)}) async-start(), calls=%async_computation.2 | async-start | bytes 4718592 | tf_op jit(solution)/shard_map/all_gather | solution.py:21
  7.9 120.8 %all-gather.3.cloned.1.call-start = ((), (), s32[]{:S(2)}) async-start(), calls=%async_computation.1 | async-start | bytes 8912896 | tf_op jit(solution)/shard_map/all_gather | solution.py:15
  12.0 167.9 %reduce-scatter.2.cloned.1.call-start = ((), (), s32[]{:S(2)}) async-start(), calls=%async_computation.3 | async-start | bytes 4718592 | tf_op jit(solution)/shard_map/reduce_scatter | solution.py:30
  128.7 7.8 %copy-start = (bf16[2048,2048]{0,1:T(8,128)(2,1)S(1)}, bf16[2048,2048]{0,1:T(8,128)(2,1)}, u32[]{:S(2)}) copy-start(bf16[2048,2048]{0,1:T(8,128)(2,1)} %all-gather.3.cloned.1.call-done) | copy-start | bytes 25165828
Sparse Core Ops, SparseCore 0:
  9.7 37.9 all-gather.4
  50.3 78.3 all-gather.2
  142.7 37.0 reduce-scatter.1
where the time goes:
time: 187 us; the launch traced here: 186 us
  waiting for transfers between devices  139 us (74%)
  local copies, waits for them, and re-layouts  15 us (8%)
  matrix products  13.8 us (7%)
  between operations  13.8 us (7%)
  other arithmetic  4.6 us (2%)
    all_gather x1, waiting for transfers between devices, side_by_side(): lax.all_gather(both, axis, axis=dim, tiled=True)  78 us
    all_gather x1, waiting for transfers between devices, on_device(): gathered = lax.all_gather(tokens, 'tp', axis=1, tiled=True)  35.6 us
    reduce_scatter x1, waiting for transfers between devices, on_device(): lax.psum_scatter(partial_value.astype(jnp.bfloat16), 'tp', scatter_dimens...  24.7 us
    unnamed x5, local copies, waits for them, and re-layouts  8.86 us
    dot_general x1, matrix products, on_device(): preact = jnp.dot(normed, up_whole, preferred_element_type=jnp.float32)  7.74 us
    transpose x1, local copies, waits for them, and re-layouts, on_device(): return (up_whole, jnp.transpose(down_whole), summed)  6.15 us
    dot_general x1, matrix products, on_device(): jnp.einsum('tf,df->td', hidden, down_whole, preferred_element_type=jnp.fl...  6.09 us
  transfers between devices with their start and end apart: 3, of which 3 were waited for; matrix products, arithmetic and copies ran while one was open for 11% of the time, Pallas kernels for 0%

commit v1 on v0

--- a/solution.py
+++ b/solution.py
@@ -18,7 +18,8 @@
 def on_device(tokens, norm_gain, up_master, down_master):
     up_local = (norm_gain[:, None] * up_master).astype(jnp.bfloat16)
     down_local = down_master.astype(jnp.bfloat16)
-    gathered = lax.all_gather(tokens, "tp", axis=1, tiled=True)
+    copies = jnp.concatenate([tokens] * lax.axis_size("tp"), axis=1)
+    gathered = lax.all_to_all(copies, "tp", 1, 1, tiled=True)
     widened = gathered.astype(jnp.float32)
     normed = (
         widened * lax.rsqrt(jnp.mean(widened * widened, axis=-1, keepdims=True) + norm_floor)

time: 187 us -> 151 us (0.81)
  waiting for transfers between devices: 139 us -> 28.1 us
  blocking collectives: 0 us -> 54.2 us
  local copies, waits for them, and re-layouts: 15 us -> 30.7 us
  other arithmetic: 4.6 us -> 8.23 us
    all_gather x1, waiting for transfers between devices: 78 us -> 3.33 us  [side_by_side(): lax.all_gather(both, axis, axis=dim, tiled=True)]
    all_to_all x0 -> x1, blocking collectives: none -> 54.2 us  [on_device(): gathered = lax.all_to_all(copies, 'tp', 1, 1, tiled=True)]
    all_gather x1 -> x0, waiting for transfers between devices: 35.6 us -> none  [on_device(): gathered = lax.all_gather(tokens, 'tp', axis=1, tiled=True)]
    all_to_all x0 -> x2, local copies, waits for them, and re-layouts: none -> 12.9 us  [on_device(): gathered = lax.all_to_all(copies, 'tp', 1, 1, tiled=True)]
    dot_general x1, matrix products: 6.09 us -> 14.5 us  [on_device(): jnp.einsum('tf,df->td', hidden, down_whole, preferred_element_type=jnp.fl...]
    dot_general x1 -> x0, matrix products: 7.74 us -> none  [on_device(): preact = jnp.dot(normed, up_whole, preferred_element_type=jnp.float32)]
    convert_element_type x0 -> x1, other arithmetic: none -> 3.25 us  [on_device(): normed = (widened * lax.rsqrt(jnp.mean(widened * widened, axis=-1, keepdi...]
    unnamed x5 -> x17, local copies, waits for them, and re-layouts: 8.86 us -> 11.6 us
  transfers between devices with their start and end apart: 3 -> 2, of which waited for: 3 -> 2; matrix products, arithmetic and copies ran while one was open for 11% -> 22% of each run, Pallas kernels for 0% -> 0%
where the time goes in v1:
time: 151 us; the launch traced here: 150 us
  blocking collectives  54.2 us (36%)
  local copies, waits for them, and re-layouts  30.7 us (20%)
  waiting for transfers between devices  28.1 us (19%)
  matrix products  14.5 us (10%)
  between operations  14.2 us (9%)
  other arithmetic  8.23 us (5%)
    all_to_all x1, blocking collectives, on_device(): gathered = lax.all_to_all(copies, 'tp', 1, 1, tiled=True)  54.2 us
    reduce_scatter x1, waiting for transfers between devices, on_device(): lax.psum_scatter(partial_value.astype(jnp.bfloat16), 'tp', scatter_dimens...  24.8 us
    dot_general x1, matrix products, on_device(): jnp.einsum('tf,df->td', hidden, down_whole, preferred_element_type=jnp.fl...  14.5 us
    all_to_all x2, local copies, waits for them, and re-layouts, on_device(): gathered = lax.all_to_all(copies, 'tp', 1, 1, tiled=True)  12.9 us
    unnamed x17, local copies, waits for them, and re-layouts  11.6 us
    transpose x1, local copies, waits for them, and re-layouts, on_device(): return (up_whole, jnp.transpose(down_whole), summed)  6.14 us
    reduce_sum x1, other arithmetic, on_device(): jnp.mean(widened * widened, axis=-1, keepdims=True) + norm_floor  3.45 us
    all_gather x1, waiting for transfers between devices, side_by_side(): lax.all_gather(both, axis, axis=dim, tiled=True)  3.33 us
  transfers between devices with their start and end apart: 2, of which 2 were waited for; matrix products, arithmetic and copies ran while one was open for 22% of the time, Pallas kernels for 0%

profile of v1, /device:TPU:0, one launch (start us, length us, event | category | flops | bytes accessed | tf_op | source)
XLA Modules:
  0.0 149.9 jit_solution(248074110774784321)
XLA Ops:
  7.2 0.0 copy-start.2
  7.2 0.0 all-gather.2.cloned.1.call-start
  7.2 1.3 copy.13
  8.5 1.2 copy.14
  9.7 0.7 multiply_convert_fusion.1
  10.4 0.8 pad_maximum_fusion
  11.2 0.0 all-gather.2.cloned.1.call-update
  11.3 0.0 reduce-scatter.2.cloned.1.call-start
  11.3 0.0 copy-done.2
  11.3 0.2 copy.15
  11.9 0.0 copy-start.1
  11.9 2.0 %copy-done.1 = bf16[1024,2048]{0,1:T(8,128)(2,1)} copy-done((bf16[1024,2048]{0,1:T(8,128)(2,1)}, bf16[1024,2048]{0,1:T(8,128)(2,1)S(1)}, u32[]{:S(2)}) %copy-start.1) | copy-done | bytes 4194328
  13.9 6.4 %copy.23 = bf16[1024,8,256]{2,0,1:T(8,128)(2,1)} copy(bf16[1024,8,256]{0,2,1:T(8,128)(2,1)} %bitcast.8) | data formatting | bytes 8388608 | tf_op jit(solution)/shard_map/all_to_all | solution.py:22
  20.3 54.2 %all_to_all.9 = bf16[1024,8,256]{2,0,1:T(8,128)(2,1)} all-to-all(bf16[1024,8,256]{2,0,1:T(8,128)(2,1)} %copy.23), channel_id=1, replica_groups=mesh['fs'=16,'tp'=8] {'tp'}, dimensions={1} | all-to-all | bytes 8388608 | tf_op jit(solution)/shard_map/all_to_all | solution.py:22
  74.6 6.4 %copy.24 = bf16[1024,8,256]{0,2,1:T(8,128)(2,1)} copy(bf16[1024,8,256]{2,0,1:T(8,128)(2,1)} %all_to_all.9) | data formatting | bytes 8388608 | tf_op jit(solution)/shard_map/all_to_all | solution.py:22
  81.0 3.4 %multiply_reduce_fusion = f32[1024]{0:T(1024)S(1)} fusion(bf16[1024,8,256]{0,2,1:T(8,128)(2,1)} %copy.24), kind=kLoop, calls=%fused_computation.2 | loop fusion | flops 6290432 | bytes 4198400 | tf_op jit(solution)/shard_map/reduce_sum | solution.py:25
  84.5 0.3 copy-done
  84.7 3.3 %fusion = bf16[1024,2048]{0,1:T(8,128)(2,1)} fusion(f32[1024]{0:T(1024)S(1)} %add_rsqrt_fusion, bf16[1024,8,256]{0,2,1:T(8,128)(2,1)S(1)} %copy-done), kind=kLoop, calls=%fused_computation.1 | loop fusion | flops 6291456 | bytes 8392704 | tf_op jit(solution)/shard_map/convert_element_type | solution.py:26
  88.0 3.3 %all-gather.2.cloned.1.call-done = bf16[2048,2048]{0,1:T(8,128)(2,1)} async-done(((bf16[128,2048]{0,1:T(8,128)(2,1)}), bf16[2048,2048]{0,1:T(8,128)(2,1)}) %all-gather.2.cloned.1.call-update) | async-done | bytes 8388624 | tf_op jit(solution)/shard_map/all_gather | solution.py:15
  91.3 14.5 %convolution_convert_fusion = bf16[1024,2048]{1,0:T(8,128)(2,1)} fusion(bf16[2048,2048]{0,1:T(8,128)(2,1)} %all-gather.2.cloned.1.call-done, bf16[1024,2048]{0,1:T(8,128)(2,1)} %fusion), kind=kOutput, calls=%fused_computation.4 | convolution fusion | flops 8595177472 | bytes 16777216 | tf_op jit(solution)/shard_map/tf,df->td/dot_general | solution.py:30
  105.8 0.0 reduce-scatter.2.cloned.1.call-update
  105.8 6.1 %slice_bitcast_fusion = (bf16[1024,2048]{1,0:T(8,128)(2,1)}, bf16[2048,1024]{0,1:T(8,128)(2,1)}) fusion(bf16[2048,2048]{0,1:T(8,128)(2,1)} %all-gather.2.cloned.1.call-done), kind=kLoop, calls=%fused_computation.6 | loop fusion | bytes 16777216 | tf_op jit(solution)/shard_map/transpose | solution.py:34
  111.9 6.4 %copy.25 = bf16[2048,1024]{1,0:T(8,128)(2,1)} copy(bf16[2048,1024]{0,1:T(8,128)(2,1)} %get-tuple-element.13) | data formatting | bytes 8388608
  118.3 24.8 %reduce-scatter.2.cloned.1.call-done = bf16[1024,256]{1,0:T(8,128)(2,1)} async-done(((bf16[1024,2048]{1,0:T(8,128)(2,1)}), bf16[1024,256]{1,0:T(8,128)(2,1)}) %reduce-scatter.2.cloned.1.call-update) | async-done | bytes 524304 | tf_op jit(solution)/shard_map/reduce_scatter | solution.py:31
  (10 shorter events, 0.3 us)
Async XLA Ops:
  7.2 4.2 %copy-start.2 = (bf16[1024,256]{1,0:T(8,128)(2,1)S(1)}, bf16[1024,256]{1,0:T(8,128)(2,1)}, u32[]{:S(2)}) copy-start(bf16[1024,256]{1,0:T(8,128)(2,1)} %param.4) | copy-start | bytes 1572868
  7.2 84.1 %all-gather.2.cloned.1.call-start = ((), (), s32[]{:S(2)}) async-start(), calls=%async_computation.2 | async-start | bytes 8912896 | tf_op jit(solution)/shard_map/all_gather | solution.py:15
  11.3 131.8 %reduce-scatter.2.cloned.1.call-start = ((), (), s32[]{:S(2)}) async-start(), calls=%async_computation.3 | async-start | bytes 4718592 | tf_op jit(solution)/shard_map/reduce_scatter | solution.py:31
  11.9 2.0 %copy-start.1 = (bf16[1024,2048]{0,1:T(8,128)(2,1)}, bf16[1024,2048]{0,1:T(8,128)(2,1)S(1)}, u32[]{:S(2)}) copy-start(bf16[1024,2048]{0,1:T(8,128)(2,1)S(1)} %constant_dynamic-update-slice_fusion) | copy-start | bytes 12582916
  81.0 3.7 %copy-start = (bf16[1024,8,256]{0,2,1:T(8,128)(2,1)S(1)}, bf16[1024,8,256]{0,2,1:T(8,128)(2,1)}, u32[]{:S(2)}) copy-start(bf16[1024,8,256]{0,2,1:T(8,128)(2,1)} %copy.24) | copy-start | bytes 12582916
Sparse Core Ops, SparseCore 0:
  11.4 79.8 all-gather.1
  105.9 37.1 reduce-scatter.1
